TPU v7x, 128 devices: a whole 4x4x4 slice. The times are simulated.
128 devices in a mesh: fs: 16 (over z, y), tp: 8 (over x, core).
Axes of the slice: x: 4, y: 4, z: 4, core: 2. Of those that a mesh axis runs over, the one named last changes fastest.
Arguments:
- tokens: bfloat16 [16384, 2048], P(('fs', 'tp')), may hold values from -6 to 6
- norm_gain: float32 [2048], replicated, may hold values from 0.1 to 1.9
- up_weight: float32 [2048, 8192], P('fs', 'tp'), may hold values from -0.125 to 0.125
- down_weight: float32 [8192, 2048], P('tp', 'fs'), may hold values from -0.0625 to 0.0625
Outputs:
- mlp_out: bfloat16 [16384, 2048], P(('fs', 'tp'))
All inputs are finite; a program needn't handle non-finite values.
Results may differ from a plain program's by a relative error of at most 0.0017.
Values may be sent and summed in bfloat16 or wider, within the bound.
A program may use at most 64 MiB of HBM per device.

v0:
```python
import jax
import jax.numpy as jnp
from jax import lax
from jax.sharding import PartitionSpec as P

epsilon = 1e-06


def taken_in(slab, axis, dim, step, start):

    def gathered(part):
        return lax.all_gather(part, axis, axis=dim, tiled=True)

    return step(start, jax.tree.map(gathered, slab), jnp.int32(0))


def on_whole(shard, axis, dim, work):
    return work(lax.all_gather(shard, axis, axis=dim, tiled=True), jnp.int32(0))


def shards(tokens, norm_gain, up_weight, down_weight):
    values = tokens.astype(jnp.float32)
    scale = lax.rsqrt(jnp.mean(values * values, axis=-1, keepdims=True) + epsilon)
    normed = (values * scale * norm_gain).astype(jnp.bfloat16)
    grouped = lax.all_gather(normed, "tp", axis=0, tiled=True)
    empty = jnp.zeros((grouped.shape[0], up_weight.shape[1]), jnp.float32)

    def add_rows(total, piece, start):
        columns = lax.dynamic_slice_in_dim(grouped, start, piece.shape[0], 1)
        return total + jnp.dot(
            columns, piece.astype(jnp.bfloat16), preferred_element_type=jnp.float32
        )

    pre = taken_in(up_weight.astype(jnp.bfloat16), "fs", 0, add_rows, empty)
    hidden = jnp.square(jax.nn.relu(pre)).astype(jnp.bfloat16)

    def project(piece, start):
        return jnp.dot(hidden, piece.astype(jnp.bfloat16), preferred_element_type=jnp.float32)

    terms = on_whole(down_weight.astype(jnp.bfloat16), "fs", 1, project)
    summed = lax.psum_scatter(terms, "tp", scatter_dimension=0, tiled=True)
    return summed.astype(jnp.bfloat16)


def solution(mesh):
    placed = (P(("fs", "tp"), None), P(), P("fs", "tp"), P("tp", "fs"))
    return jax.shard_map(
        shards, mesh=mesh, in_specs=placed, out_specs=P(("fs", "tp"), None), check_vma=False
    )
```

profile of v0, /device:TPU:1, one launch (start us, length us, event | category | flops | bytes accessed | tf_op | source)
XLA Modules:
  0.0 232.5 jit_solution(14041995372060814346)
XLA Ops:
  6.5 0.0 all-gather.4.cloned.1.call-start
  6.5 1.2 fusion
  7.8 2.0 fusion.2
  9.8 0.0 all-gather.4.cloned.1.call-update
  9.8 0.0 all-gather.6.cloned.1.call-start
  9.9 1.8 convert_element_type.20
  11.7 0.0 all-gather.6.cloned.1.call-update
  11.7 0.0 all-gather.8.cloned.1.call-start
  11.7 1.8 convert_element_type.22
  13.5 0.0 all-gather.8.cloned.1.call-update
  13.5 0.0 reduce-scatter.2.cloned.1.call-start
  13.6 32.0 %all-gather.4.cloned.1.call-done = bf16[1024,2048]{1,0:T(8,128)(2,1)} async-done(((bf16[128,2048]{1,0:T(8,128)(2,1)}), bf16[1024,2048]{1,0:T(8,128)(2,1)}) %all-gather.4.cloned.1.call-update) | async-done | bytes 4194320 | tf_op jit(solution)/shard_map/all_gather | solution.py:25
  45.6 53.1 %all-gather.6.cloned.1.call-done = bf16[2048,1024]{1,0:T(8,128)(2,1)} async-done(((bf16[128,1024]{1,0:T(8,128)(2,1)}), bf16[2048,1024]{1,0:T(8,128)(2,1)}) %all-gather.6.cloned.1.call-update) | async-done | bytes 4194320 | tf_op jit(solution)/shard_map/all_gather | solution.py:12
  98.7 57.5 %all-gather.8.cloned.1.call-done = bf16[1024,2048]{1,0:T(8,128)(2,1)} async-done(((bf16[1024,128]{1,0:T(8,128)(2,1)}), bf16[1024,2048]{1,0:T(8,128)(2,1)}) %all-gather.8.cloned.1.call-update) | async-done | bytes 4194320 | tf_op jit(solution)/shard_map/all_gather | solution.py:18
  156.2 15.0 %fusion.3 = f32[1024,2048]{1,0:T(8,128)} fusion(bf16[1024,2048]{1,0:T(8,128)(2,1)} %all-gather.8.cloned.1.call-done, bf16[1024,2048]{1,0:T(8,128)(2,1)} %all-gather.4.cloned.1.call-done, bf16[2048,1024]{1,0:T(8,128)(2,1)} %all-gather.6.cloned.1.call-done), kind=kOutput, calls=%fused_computation.6 | convolution fusion | flops 8593080320 | bytes 20971520 | tf_op jit(solution)/shard_map/dot_general | solution.py:38
  171.2 0.0 reduce-scatter.2.cloned.1.call-update
  171.2 52.6 %reduce-scatter.2.cloned.1.call-done = f32[128,2048]{1,0:T(8,128)} async-done(((f32[1024,2048]{1,0:T(8,128)}), f32[128,2048]{1,0:T(8,128)}) %reduce-scatter.2.cloned.1.call-update) | async-done | bytes 1048592 | tf_op jit(solution)/shard_map/reduce_scatter | solution.py:41
  223.9 2.1 convert_element_type.23
  (1 shorter events, 0.0 us)
Async XLA Ops:
  6.5 39.1 %all-gather.4.cloned.1.call-start = ((), (), s32[]{:S(2)}) async-start(), calls=%async_computation.1 | async-start | bytes 4718592 | tf_op jit(solution)/shard_map/all_gather | solution.py:25
  9.8 88.9 %all-gather.6.cloned.1.call-start = ((), (), s32[]{:S(2)}) async-start(), calls=%async_computation.2 | async-start | bytes 4456448 | tf_op jit(solution)/shard_map/all_gather | solution.py:12
  11.7 144.5 %all-gather.8.cloned.1.call-start = ((), (), s32[]{:S(2)}) async-start(), calls=%async_computation.3 | async-start | bytes 4456448 | tf_op jit(solution)/shard_map/all_gather | solution.py:18
  13.5 210.4 %reduce-scatter.2.cloned.1.call-start = ((), (), s32[]{:S(2)}) async-start(), calls=%async_computation.4 | async-start | bytes 9437184 | tf_op jit(solution)/shard_map/reduce_scatter | solution.py:41
Sparse Core Ops, SparseCore 0:
  9.9 35.6 all-gather.3
  47.7 50.9 all-gather.5
  100.8 55.3 all-gather.7
  171.4 52.4 reduce-scatter.1
where the time goes:
time: 233 us
  waiting for transfers between devices  195 us (84%)
  matrix products  15 us (6%)
  between operations  13.1 us (6%)
  other arithmetic  8.9 us (4%)
    all_gather x1, waiting for transfers between devices, on_whole(): return work(lax.all_gather(shard, axis, axis=dim, tiled=True), jnp.int32(0))  57.5 us
    all_gather x1, waiting for transfers between devices, gathered(): return lax.all_gather(part, axis, axis=dim, tiled=True)  53.1 us
    reduce_scatter x1, waiting for transfers between devices, shards(): summed = lax.psum_scatter(terms, 'tp', scatter_dimension=0, tiled=True)  52.6 us
    all_gather x1, waiting for transfers between devices, shards(): grouped = lax.all_gather(normed, 'tp', axis=0, tiled=True)  32 us
    dot_general x1, matrix products, project(): jnp.dot(hidden, piece.astype(jnp.bfloat16), preferred_element_type=jnp.fl...  15 us
  transfers between devices with their start and end apart: 4, of which 4 were waited for; matrix products, arithmetic and copies ran while one was open for 2% of the time, Pallas kernels for 0%

commit v1 on v0

--- a/solution.py
+++ b/solution.py
@@ -22,7 +22,11 @@
     values = tokens.astype(jnp.float32)
     scale = lax.rsqrt(jnp.mean(values * values, axis=-1, keepdims=True) + epsilon)
     normed = (values * scale * norm_gain).astype(jnp.bfloat16)
-    grouped = lax.all_gather(normed, "tp", axis=0, tiled=True)
+    length = lax.axis_size("tp")
+    repeats = [length if d == 0 else 1 for d in range(normed.ndim)]
+    grouped = lax.all_to_all(
+        jnp.tile(normed, repeats), "tp", split_axis=0, concat_axis=0, tiled=True
+    )
     empty = jnp.zeros((grouped.shape[0], up_weight.shape[1]), jnp.float32)
 
     def add_rows(total, piece, start):

time: 233 us -> 198 us (0.85)
  waiting for transfers between devices: 195 us -> 107 us
  blocking collectives: 0 us -> 54.3 us
    all_to_all x0 -> x1, blocking collectives: none -> 54.3 us  [shards(): lax.all_to_all(jnp.tile(normed, repeats), 'tp', split_axis=0, concat_axis...]
    all_gather x1, waiting for transfers between devices: 53.1 us -> 0.01 us  [gathered(): return lax.all_gather(part, axis, axis=dim, tiled=True)]
    all_gather x1 -> x0, waiting for transfers between devices: 32 us -> none  [shards(): grouped = lax.all_gather(normed, 'tp', axis=0, tiled=True)]
    all_gather x1, waiting for transfers between devices: 57.5 us -> 54 us  [on_whole(): return work(lax.all_gather(shard, axis, axis=dim, tiled=True), jnp.int32(0))]
  transfers between devices with their start and end apart: 4 -> 3, of which waited for: 4 -> 2; matrix products, arithmetic and copies ran while one was open for 2% -> 2% of each run, Pallas kernels for 0% -> 0%
where the time goes in v1:
time: 198 us
  waiting for transfers between devices  107 us (54%)
  blocking collectives  54.3 us (27%)
  matrix products  15 us (8%)
  between operations  13.1 us (7%)
  other arithmetic  8.1 us (4%)
    all_to_all x1, blocking collectives, shards(): lax.all_to_all(jnp.tile(normed, repeats), 'tp', split_axis=0, concat_axis...  54.3 us
    all_gather x1, waiting for transfers between devices, on_whole(): return work(lax.all_gather(shard, axis, axis=dim, tiled=True), jnp.int32(0))  54 us
    reduce_scatter x1, waiting for transfers between devices, shards(): summed = lax.psum_scatter(terms, 'tp', scatter_dimension=0, tiled=True)  52.6 us
    dot_general x1, matrix products, project(): jnp.dot(hidden, piece.astype(jnp.bfloat16), preferred_element_type=jnp.fl...  15 us
  transfers between devices with their start and end apart: 3, of which 2 were waited for; matrix products, arithmetic and copies ran while one was open for 2% of the time, Pallas kernels for 0%

profile of v1, /device:TPU:1, one launch (start us, length us, event | category | flops | bytes accessed | tf_op | source)
XLA Modules:
  0.0 197.8 jit_solution(489317753236248873)
XLA Ops:
  6.5 0.0 all-gather.3.cloned.1.call-start
  6.5 1.8 convert_element_type.20
  8.3 0.0 all-gather.3.cloned.1.call-update
  8.3 0.0 all-gather.5.cloned.1.call-start
  8.4 1.8 convert_element_type.22
  10.2 0.0 all-gather.5.cloned.1.call-update
  10.2 0.0 reduce-scatter.2.cloned.1.call-start
  10.2 1.2 fusion
  11.5 1.2 fusion.2
  12.7 0.5 tile.2
  13.2 54.3 %all_to_all.9 = bf16[8,128,2048]{2,1,0:T(8,128)(2,1)} all-to-all(bf16[8,128,2048]{2,1,0:T(8,128)(2,1)S(1)} %tile.2), channel_id=1, replica_groups=mesh['fs'=16,'tp'=8] {'tp'}, dimensions={0} | all-to-all | bytes 8388608 | tf_op jit(solution)/shard_map/all_to_all | solution.py:27
  67.6 0.0 all-gather.3.cloned.1.call-done
  67.6 54.0 %all-gather.5.cloned.1.call-done = bf16[1024,2048]{1,0:T(8,128)(2,1)} async-done(((bf16[1024,128]{1,0:T(8,128)(2,1)}), bf16[1024,2048]{1,0:T(8,128)(2,1)}) %all-gather.5.cloned.1.call-update) | async-done | bytes 4194320 | tf_op jit(solution)/shard_map/all_gather | solution.py:18
  121.6 15.0 %fusion.3 = f32[1024,2048]{1,0:T(8,128)} fusion(bf16[1024,2048]{1,0:T(8,128)(2,1)} %all-gather.5.cloned.1.call-done, bf16[1024,2048]{1,0:T(8,128)(2,1)} %bitcast.4, bf16[2048,1024]{1,0:T(8,128)(2,1)} %all-gather.3.cloned.1.call-done), kind=kOutput, calls=%fused_computation.6 | convolution fusion | flops 8593080320 | bytes 20971520 | tf_op jit(solution)/shard_map/dot_general | solution.py:42
  136.6 0.0 reduce-scatter.2.cloned.1.call-update
  136.6 52.6 %reduce-scatter.2.cloned.1.call-done = f32[128,2048]{1,0:T(8,128)} async-done(((f32[1024,2048]{1,0:T(8,128)}), f32[128,2048]{1,0:T(8,128)}) %reduce-scatter.2.cloned.1.call-update) | async-done | bytes 1048592 | tf_op jit(solution)/shard_map/reduce_scatter | solution.py:45
  189.2 2.1 %convert_element_type.23 = bf16[128,2048]{1,0:T(8,128)(2,1)} convert(f32[128,2048]{1,0:T(8,128)} %reduce-scatter.2.cloned.1.call-done) | non-fusion elementwise | flops 262144 | bytes 1572864 | tf_op jit(solution)/shard_map/convert_element_type | solution.py:46
  (1 shorter events, 0.0 us)
Async XLA Ops:
  6.5 61.0 %all-gather.3.cloned.1.call-start = ((), (), s32[]{:S(2)}) async-start(), calls=%async_computation.2 | async-start | bytes 4456448 | tf_op jit(solution)/shard_map/all_gather | solution.py:12
  8.3 113.2 %all-gather.5.cloned.1.call-start = ((), (), s32[]{:S(2)}) async-start(), calls=%async_computation.3 | async-start | bytes 4456448 | tf_op jit(solution)/shard_map/all_gather | solution.py:18
  10.2 179.1 %reduce-scatter.2.cloned.1.call-start = ((), (), s32[]{:S(2)}) async-start(), calls=%async_computation.4 | async-start | bytes 9437184 | tf_op jit(solution)/shard_map/reduce_scatter | solution.py:45
Sparse Core Ops, SparseCore 0:
  9.5 54.5 all-gather.2
  66.2 55.3 all-gather.4
  136.7 52.4 reduce-scatter.1
